TPU v7x, 256 devices: a whole 4x4x8 slice. The times are simulated.
256 devices in a mesh: fs: 32 (over z, y), tp: 8 (over x, core).
Axes of the slice: x: 4, y: 4, z: 8, core: 2. Of those that a mesh axis runs over, the one named last changes fastest.
Arguments:
- cotangent: bfloat16 [32768, 4096], P(('fs', 'tp')), may hold values from -24 to 24
- gate_pre: bfloat16 [32768, 6144], P('fs', 'tp'), may hold values from -8 to 8
- up_pre: bfloat16 [32768, 6144], P('fs', 'tp'), may hold values from -6 to 6
- down_weight: bfloat16 [4096, 6144], P('fs', 'tp'), may hold values from -0.078125 to 0.078125
Outputs:
- gate_grad: bfloat16 [32768, 6144], P('fs', 'tp')
- up_grad: bfloat16 [32768, 6144], P('fs', 'tp')
- down_grad: float32 [4096, 6144], P('fs', 'tp')
All inputs are finite; a program needn't handle non-finite values.
Results may differ from a plain program's by a relative error of at most 0.0027.
Values may be sent and summed in bfloat16 or wider, within the bound.
A program may use at most 128 MiB of HBM per device.

v0:
```python
import math

import jax
import jax.numpy as jnp
from jax import lax
from jax.sharding import Mesh
from jax.sharding import PartitionSpec as P

FS = ("fs_0", "fs_1")
FS_TP = ("fs_0", "fs_1", "tp")


def sum_by_axis(total, axes):
    for axis in axes:
        total = lax.psum_scatter(total, axis, scatter_dimension=0, tiled=True)
    return total


def local(cotangent, gate_pre, up_pre, down_weight):
    token_total = gate_pre.shape[0] * lax.axis_size(FS)
    grad_scale = 0.5 / math.sqrt(token_total)
    gathered = lax.all_gather(cotangent, "tp", axis=0, tiled=True)
    gate_values = gate_pre.astype(jnp.float32)
    up_values = up_pre.astype(jnp.float32)
    sigmoid_gate = jax.nn.sigmoid(gate_values)
    silu_gate = gate_values * sigmoid_gate
    hidden = (silu_gate * up_values).astype(jnp.bfloat16)
    columns = gathered
    contracted = jnp.dot(
        columns,
        lax.all_gather(down_weight, FS, axis=0, tiled=True),
        preferred_element_type=jnp.float32,
    )
    columns = gathered
    down_grad = (
        sum_by_axis(
            lax.dot_general(
                columns, hidden, (((0,), (0,)), ((), ())), preferred_element_type=jnp.float32
            ),
            FS,
        )
        * grad_scale
    )
    hidden_grad = 0.5 * contracted
    up_grad = (hidden_grad * silu_gate).astype(jnp.bfloat16)
    gate_grad = (
        hidden_grad * up_values * sigmoid_gate * (1.0 + gate_values * (1.0 - sigmoid_gate))
    ).astype(jnp.bfloat16)
    return (gate_grad, up_grad, down_grad)


def solution(mesh):
    torus = Mesh(mesh.devices.reshape(8, 4, mesh.shape["tp"]), ("fs_0", "fs_1", "tp"))
    return jax.shard_map(
        local,
        mesh=torus,
        in_specs=(P(FS_TP, None), P(FS, "tp"), P(FS, "tp"), P(FS, "tp")),
        out_specs=(P(FS, "tp"), P(FS, "tp"), P(FS, "tp")),
        check_vma=False,
    )
```

profile of v0, /device:TPU:8, one launch (start us, length us, event | category | flops | bytes accessed | tf_op | source)
XLA Modules:
  0.0 293.6 jit_solution(12159855987498780870)
XLA Ops:
  8.0 0.0 all-gather.3.cloned.1.call-start
  8.0 0.7 all-gather.3.cloned.1.call-update
  8.7 0.0 reduce-scatter.3.cloned.1.call-start
  8.8 57.0 %all-gather.3.cloned.1.call-done = bf16[1024,4096]{1,0:T(8,128)(2,1)} async-done(((bf16[128,4096]{1,0:T(8,128)(2,1)}), bf16[1024,4096]{1,0:T(8,128)(2,1)}) %all-gather.3.cloned.1.call-update) | async-done | bytes 8388624 | tf_op jit(solution)/shard_map/all_gather | solution.py:22
  65.8 13.7 %convolution_bitcast_fusion = f32[4096,768]{0,1:T(8,128)} fusion(bf16[1024,4096]{1,0:T(8,128)(2,1)} %all-gather.3.cloned.1.call-done, bf16[1024,768]{1,0:T(8,128)(2,1)} %param.6, bf16[1024,768]{1,0:T(8,128)(2,1)} %param.5), kind=kOutput, calls=%fused_computation | convolution fusion | flops 6448742400 | bytes 24117248 | tf_op jit(solution)/shard_map/dot_general | solution.py:37
  79.5 0.0 copy-start
  79.5 0.0 copy-start.1
  79.5 0.0 reduce-scatter.3.cloned.1.call-update
  79.5 0.0 all-gather.5.cloned.1.call-start
  79.6 0.5 all-gather.5.cloned.1.call-update
  80.1 0.0 reduce-scatter.5.cloned.1.call-start
  80.1 141.7 %reduce-scatter.3.cloned.1.call-done = f32[512,768]{0,1:T(8,128)} async-done(((f32[4096,768]{0,1:T(8,128)}), f32[512,768]{0,1:T(8,128)}) %reduce-scatter.3.cloned.1.call-update) | async-done | bytes 1572880 | tf_op jit(solution)/shard_map/reduce_scatter | solution.py:15
  221.8 0.0 reduce-scatter.5.cloned.1.call-update
  221.8 49.8 %all-gather.5.cloned.1.call-done = bf16[4096,768]{1,0:T(8,128)(2,1)} async-done(((bf16[128,768]{1,0:T(8,128)(2,1)}), bf16[4096,768]{1,0:T(8,128)(2,1)}) %all-gather.5.cloned.1.call-update) | async-done | bytes 6291472 | tf_op jit(solution)/shard_map/all_gather | solution.py:31
  271.6 0.0 copy-done
  271.6 0.0 copy-done.1
  271.6 12.9 %multiply_convert_fusion = (bf16[1024,768]{1,0:T(8,128)(2,1)}, bf16[1024,768]{1,0:T(8,128)(2,1)}) fusion(bf16[1024,768]{1,0:T(8,128)(2,1)S(1)} %copy-done, bf16[1024,768]{1,0:T(8,128)(2,1)S(1)} %copy-done.1, bf16[1024,4096]{1,0:T(8,128)(2,1)} %all-gather.3.cloned.1.call-done, bf16[4096,768]{1,0:T(8,128)(2,1)} %all-gather.5.cloned.1.call-done), kind=kOutput, calls=%fused_computation.14 | convolution fusion | flops 6455033856 | bytes 20971520 | tf_op jit(solution)/shard_map/dot_general | solution.py:29
  284.6 0.0 reduce-scatter.5.cloned.1.call-done
  284.6 1.0 broadcast_multiply_fusion
  285.6 0.9 copy.7
Async XLA Ops:
  8.0 57.8 %all-gather.3.cloned.1.call-start = ((), (), s32[]{:S(2)}) async-start(), calls=%async_computation.2 | async-start | bytes 9437184 | tf_op jit(solution)/shard_map/all_gather | solution.py:22
  8.7 213.1 %reduce-scatter.3.cloned.1.call-start = ((), (), s32[]{:S(2)}) async-start(), calls=%async_computation.4 | async-start | bytes 14155776 | tf_op jit(solution)/shard_map/reduce_scatter | solution.py:15
  79.5 192.1 %copy-start = (bf16[1024,768]{1,0:T(8,128)(2,1)S(1)}, bf16[1024,768]{1,0:T(8,128)(2,1)}, u32[]{:S(2)}) copy-start(bf16[1024,768]{1,0:T(8,128)(2,1)} %param.5) | copy-start | bytes 4718596
  79.5 192.1 %copy-start.1 = (bf16[1024,768]{1,0:T(8,128)(2,1)S(1)}, bf16[1024,768]{1,0:T(8,128)(2,1)}, u32[]{:S(2)}) copy-start(bf16[1024,768]{1,0:T(8,128)(2,1)} %param.6) | copy-start | bytes 4718596
  79.5 192.1 %all-gather.5.cloned.1.call-start = ((), (), s32[]{:S(2)}) async-start(), calls=%async_computation.3 | async-start | bytes 6488064 | tf_op jit(solution)/shard_map/all_gather | solution.py:31
  80.1 204.5 %reduce-scatter.5.cloned.1.call-start = ((), (), s32[]{:S(2)}) async-start(), calls=%async_computation.5 | async-start | bytes 1966080 | tf_op jit(solution)/shard_map/reduce_scatter | solution.py:15
Sparse Core Ops, SparseCore 0:
  10.7 55.0 all-gather.2
  79.6 142.1 reduce-scatter.2
  224.4 43.3 reduce-scatter.4
Sparse Core Ops, SparseCore 1:
  82.6 189.0 all-gather.4
where the time goes:
time: 295 us; the launch traced here: 294 us
  waiting for transfers between devices  250 us (85%)
  matrix products  26.7 us (9%)
  between operations  15.2 us (5%)
    reduce_scatter x2, waiting for transfers between devices, sum_by_axis(): total = lax.psum_scatter(total, axis, scatter_dimension=0, tiled=True)  142 us
    all_gather x1, waiting for transfers between devices, local(): gathered = lax.all_gather(cotangent, 'tp', axis=0, tiled=True)  57 us
    all_gather x1, waiting for transfers between devices, local(): lax.all_gather(down_weight, FS, axis=0, tiled=True)  49.8 us
    dot_general x1, matrix products, local(): lax.dot_general(columns, hidden, (((0,), (0,)), ((), ())), preferred_elem...  13.7 us
    dot_general x1, matrix products, local(): jnp.dot(columns, lax.all_gather(down_weight, FS, axis=0, tiled=True), pre...  12.9 us
  transfers between devices with their start and end apart: 4, of which 3 were waited for; matrix products, arithmetic and copies ran while one was open for 4% of the time, Pallas kernels for 0%

commit v1 on v0

v1 whole, which is shorter than its diff:
```python
import math

import jax
import jax.numpy as jnp
from jax import lax
from jax.experimental import pallas as pl
from jax.experimental.pallas import tpu as pltpu
from jax.sharding import Mesh
from jax.sharding import PartitionSpec as P

ORDER = [
    0, 77, 78, 82, 1, 107, 97, 87, 39, 96, 59, 86, 106, 21, 43, 116, 35, 117, 73, 5, 88, 92, 27, 60, 65, 22,
    69, 31, 2, 45, 7, 40, 9, 47, 36, 74, 44, 6, 80, 84, 98, 83, 23, 61, 46, 28, 66, 8, 102, 32, 70, 49, 11,
    51, 13, 3, 41, 90, 94, 79, 48, 10, 24, 62, 85, 108, 112, 37, 75, 50, 12, 33, 67, 100, 52, 29, 71, 14, 15,
    53, 55, 81, 104, 17, 89, 93, 4, 42, 25, 63, 118, 188, 119, 185, 103, 143, 99, 138, 196, 193, 167, 139,
    189, 155, 162, 186, 110, 114, 179, 109, 113, 197, 163, 194, 68, 150, 57, 19, 76, 151, 72, 91, 95, 175, 64,
    140, 190, 187, 120, 105, 204, 201, 101, 145, 121, 205, 202, 164, 157, 169, 174, 156, 26, 152, 198, 144,
    122, 212, 195, 115, 123, 209, 219, 111, 181, 180, 38, 30, 34, 216, 168, 141, 220, 192, 124, 203, 206, 125,
    191, 217, 226, 158, 165, 210, 146, 227, 224, 214, 199, 211, 182, 221, 153, 218, 233, 170, 142, 223, 213,
    230, 208, 228, 200, 207, 231, 234, 176, 16, 147, 240, 166, 20, 58, 159, 154, 18, 235, 171, 225, 56, 215,
    232, 54, 222, 237, 177, 241, 148, 149, 183, 160, 242, 172, 238, 229, 128, 136, 236, 137, 178, 239, 133,
    132, 161, 173, 131, 129, 134, 126, 130, 127, 135, 243, 184,
]

NZ, NY, NX = 8, 4, 4
F32, BF16 = jnp.float32, jnp.bfloat16
BOTH = (1, -1)
ZORDER = [4, 3, -3, 2, -2, 1, -1, 0]
YORDER = [2, 1, -1, 0]
WA = 48
GA, GA_CUT, GB_CUT = 336, 176, 560
GROWS = {("A", 0): (0, GA_CUT), ("A", 1): (GA_CUT, GA), ("B", 0): (GA, GB_CUT), ("B", 1): (GB_CUT, 768)}
LINKS = [(a, s) for a in "zyx" for s in BOTH] + [("c", 1)]
BARRIER = len(LINKS)


def nz(v):
    return (v + 3) % 8 - 3


def ny(v):
    return (v + 1) % 4 - 1


def block_at(rz, ry):
    return ZORDER.index(nz(rz)) * 4 + YORDER.index(ny(ry))


def grows(part, half):
    if half is None:
        return GROWS[part, 0][0], GROWS[part, 1][1]
    return GROWS[part, half]


def step(rz, ry, axis, sign):
    return (nz(rz - sign), ry) if axis == "z" else (rz, ny(ry - sign))


class Tasks:
    def __init__(self, c):
        self.c = c
        self.tasks = []
        self.message = {}
        self.index = {}
        self.rows = {}
        self.total_rows = {BF16: 0, F32: 0}
        self.build()

    def task(self, name, needs, time, function=None, message=None):
        assert name not in self.index, name
        self.index[name] = len(self.tasks)
        if message:
            assert message[0] not in self.message
            self.message[message[0]] = len(self.message)
        self.tasks.append((name, tuple(needs), time, function, message))

    def weight(self, rz, ry, part, half, axis, sign, needs):
        tz, ty = step(rz, ry, axis, sign)
        r0, r1 = (0, WA) if part == "A" else (WA, 128)
        c0, c1 = (0, 768) if half is None else ((0, 384), (384, 768))[half]

        def at(z, y):
            b = block_at(z, y) * 128
            return lambda: self.c.w.at[pl.ds(b + r0, r1 - r0), pl.ds(c0, c1 - c0)]

        name = ("W", part, axis, sign, tz, ty)
        link, size = (axis, sign), (r1 - r0) * (c1 - c0) * 2
        self.task(("t",) + name, needs, 0.0, None, (name, link, size, at(rz, ry), at(tz, ty)))

    def cot(self, kind, piece, link, dx, half, needs):
        c = self.c
        h0, h1 = (0, 128) if half is None else ((0, 64), (64, 128))[half]

        def at():
            return c.cot.at[pl.ds(c.token_row(dx) + h0, h1 - h0), pl.ds(piece * 1024, 1024)]

        name = ("C", kind, piece, link)
        self.task(("t",) + name, needs, 0.0, None, (name, link, (h1 - h0) * 2048, at, at))

    def gradient(self, cls, part, half, axis, sign, rz, ry, needs, ins, kind):
        c = self.c
        tz, ty = step(rz, ry, axis, sign)
        name = (cls, half, sign, tz, ty)
        r0, r1 = grows(part, half)
        self.rows[name] = (kind, r0, r1, self.total_rows[kind])
        self.total_rows[kind] += r1 - r0
        self.task(
            ("t",) + name,
            list(needs) + list(ins),
            0.03,
            lambda: c.add(part, r0, r1, block_at(rz, ry), ins, name),
            (name, (axis, sign), (r1 - r0) * 128 * (2 if kind == BF16 else 4), lambda: c.slot("send", name), lambda: c.slot("recv", name)),
        )

    def build(self):
        c, weight, cot, task, gradient = self.c, self.weight, self.cot, self.task, self.gradient
        task("start", [], 2.5, lambda: c.start())
        start = ["start"]
        arrived = []
        for s in BOTH:
            h = 0 if s == 1 else 1
            weight(0, 0, "B", None, "z", s, start)
            for hop in (1, 2, 3):
                weight(-s * hop, 0, "B", h if hop == 3 else None, "z", s, [("W", "B", "z", s, -s * hop, 0)])
            for rz in [0, -1, 1, -2, 2, -3, 3, 4]:
                if rz == 0:
                    needs = start
                elif rz == 4:
                    needs = [("W", "B", "z", t, 4, 0) for t in BOTH]
                else:
                    needs = [("W", "B", "z", 1 if rz < 0 else -1, rz, 0)]
                weight(rz, 0, "B", None, "y", s, needs)
                weight(rz, -s, "B", h, "y", s, [("W", "B", "y", s, rz, -s)])
                arrived.append(("W", "B", "y", s, rz, 2))
            weight(0, 0, "A", None, "y", s, start)
            weight(0, -s, "A", h, "y", s, [("W", "A", "y", s, 0, -s)])
            for ry in YORDER:
                if ry == 0:
                    needs = start
                elif ry == 2:
                    needs = [("W", "A", "y", t, 0, 2) for t in BOTH]
                else:
                    needs = [("W", "A", "y", -ry, 0, ry)]
                weight(0, ry, "A", None, "z", s, needs)
                for hop in (1, 2, 3):
                    weight(-s * hop, ry, "A", h if hop == 3 else None, "z", s, [("W", "A", "z", s, -s * hop, ry)])
                arrived.append(("W", "A", "z", s, 4, ry))
        for k in range(4):
            task(("load", k), start, 0.0, lambda k=k: c.wait_cot_load(k))
            for s in BOTH:
                h = 0 if s == 1 else 1
                own = ("C", "own", k, ("x", s))
                cot("own", k, ("x", s), 0, None, [("load", k)])
                cot("forward", k, ("x", s), -s, h, [own])
                cot("side%d" % s, k, ("c", 1), -s, None, [own])
                cot("far%d" % s, k, ("c", 1), -2 * s, h, [("C", "forward", k, ("x", s))])
            cot("own", k, ("c", 1), 0, None, [("load", k)])
        task("hidden", start, 1.8, lambda: c.hidden())
        for i, rz in enumerate(ZORDER):
            k = i // 2
            pieces = [("C", kind, k, ("c", 1)) for kind in ("own", "side1", "side-1", "far1", "far-1")]
            pieces += [("C", kind, k, ("x", s)) for kind in ("own", "forward") for s in BOTH]
            task(("down", rz), ["hidden", ("load", k)] + pieces, 0.98, lambda i=i: c.down_product(i))
        for i in range(12):
            task(("hg", i), arrived + [("down", 0), ("down", 4), ("down", -3), ("down", -2)], 0.65, lambda i=i: c.hidden_grad(i))
        for ry in YORDER:
            for s in BOTH:
                h = 0 if s == 1 else 1
                gradient("A1", "A", h, "z", s, 4, ry, [("down", 4)], [], BF16)
                gradient("A1", "A", 1 - h, "z", s, 3 * s, ry, [("down", 3 * s)], [], BF16)
                gradient("A1", "A", h, "z", s, 3 * s, ry, [("down", 3 * s)], [("A1", h, s, 3 * s, ry)], BF16)
                gradient("A1", "A", None, "z", s, 2 * s, ry, [("down", 2 * s)], [("A1", v, s, 2 * s, ry) for v in (0, 1)], BF16)
                gradient("A1", "A", None, "z", s, s, ry, [("down", s)], [("A1", None, s, s, ry)], BF16)
            ins = [("A1", None, s, 0, ry) for s in BOTH]
            if ry == 2:
                for s in BOTH:
                    gradient("A2", "A", 0 if s == 1 else 1, "y", s, 0, 2, [("down", 0)], ins, F32)
            elif ry:
                h = 0 if ry == 1 else 1
                gradient("A2", "A", 1 - h, "y", ry, 0, ry, [("down", 0)], ins, F32)
                gradient("A2", "A", h, "y", ry, 0, ry, [("down", 0)], ins + [("A2", h, ry, 0, ry)], F32)
            else:
                ins = ins + [("A2", v, s, 0, 0) for s in BOTH for v in (0, 1)]
                task("finalA", ins + [("down", 0)], 0.05, lambda ins=ins: c.add("A", *grows("A", None), block_at(0, 0), ins, None))
        for rz in ZORDER:
            for s in BOTH:
                h = 0 if s == 1 else 1
                gradient("B1", "B", h, "y", s, rz, 2, [("down", rz)], [], BF16)
                gradient("B1", "B", 1 - h, "y", s, rz, s, [("down", rz)], [], BF16)
                gradient("B1", "B", h, "y", s, rz, s, [("down", rz)], [("B1", h, s, rz, s)], BF16)
            ins = [("B1", v, s, rz, 0) for s in BOTH for v in (0, 1)]
            if rz == 4:
                for s in BOTH:
                    gradient("B2", "B", 0 if s == 1 else 1, "z", s, 4, 0, [("down", 4)], ins, BF16)
            elif rz:
                s = 1 if rz > 0 else -1
                h = 0 if s == 1 else 1
                if abs(rz) == 3:
                    gradient("B2", "B", 1 - h, "z", s, rz, 0, [("down", rz)], ins, BF16)
                    gradient("B2", "B", h, "z", s, rz, 0, [("down", rz)], ins + [("B2", h, s, rz, 0)], BF16)
                elif abs(rz) == 2:
                    gradient("B2", "B", None, "z", s, rz, 0, [("down", rz)], ins + [("B2", v, s, rz, 0) for v in (0, 1)], BF16)
                else:
                    gradient("B2", "B", None, "z", s, rz, 0, [("down", rz)], ins + [("B2", None, s, rz, 0)], F32)
            else:
                ins = ins + [("B2", None, s, 0, 0) for s in BOTH]
                task("finalB", ins + [("down", 0)], 0.05, lambda ins=ins: c.add("B", *grows("B", None), block_at(0, 0), ins, None))


class Nothing:
    pass


class Kernel:
    def __init__(self, refs, scale):
        self.__dict__.update(refs)
        self.scale = scale
        self.z, self.y, self.x, self.core = (lax.axis_index(a) for a in ("z", "y", "x", "core"))
        self.pending = []

    def token_row(self, dx):
        return pl.multiple_of(lax.rem(self.x + dx + NX, NX) * 256 + self.core * 128, 128)

    def device(self, link):
        axis, sign = link
        if axis == "c":
            return {"core": 1 - self.core}
        size = {"z": NZ, "y": NY, "x": NX}[axis]
        return {axis: lax.rem(getattr(self, axis) + sign + size, size)}

    def local(self, src, dst, sem):
        copy = pltpu.make_async_copy(src, dst, self.lsem.at[sem])
        copy.start()
        return copy

    def start(self):
        barrier = pltpu.get_barrier_semaphore()
        for link in LINKS:
            pl.semaphore_signal(barrier, inc=1, device_id=self.device(link), device_id_type=pl.DeviceIdType.MESH)
        w_load = self.local(self.w_hbm, self.w.at[pl.ds(block_at(0, 0) * 128, 128)], 0)
        self.cot_loads = []
        own = self.token_row(0)
        for i, rz in enumerate(ZORDER):
            for j, ry in enumerate(YORDER):
                col = (lax.rem(self.z + rz + NZ, NZ) * NY + lax.rem(self.y + ry + NY, NY)) * 128
                b = i * 4 + j
                source = self.cot_hbm.at[:, pl.ds(pl.multiple_of(col, 128), 128)]
                self.cot_loads.append(self.local(source, self.cot.at[pl.ds(own, 128), pl.ds(b * 128, 128)], 3 + b))
        self.g_load = self.local(self.gate_hbm, self.gate, 1)
        self.u_load = self.local(self.up_hbm, self.up, 2)
        pl.semaphore_wait(barrier, BARRIER)
        w_load.wait()

    def wait_cot_load(self, k):
        for b in range(8 * k, 8 * k + 8):
            self.cot_loads[b].wait()

    def hidden(self):
        self.g_load.wait()
        self.u_load.wait()

        def body(i, carry):
            rows = pl.ds(pl.multiple_of(i * 128, 128), 128)
            for n in range(6):
                cols = pl.ds(n * 128, 128)
                g = self.gate[rows, cols].astype(F32)
                u = self.up[rows, cols].astype(F32)
                s = jax.nn.sigmoid(g)
                silu = g * s
                self.ht[cols, rows] = (silu * u).T.astype(BF16)
                self.to_up[rows, cols] = 0.5 * silu
                self.to_gate[rows, cols] = 0.5 * (u * s * (1.0 + g * (1.0 - s)))
            return carry

        lax.fori_loop(0, 8, body, 0)

    def down_product(self, z):
        for half in range(2):
            b = z * 4 + half * 2
            res = jnp.dot(self.ht[...], self.cot[:, pl.ds(b * 128, 256)], preferred_element_type=F32)
            self.part[b] = res[:, :128]
            self.part[b + 1] = res[:, 128:]

    def slot(self, side, name):
        kind, r0, r1, offset = self.rows[name]
        return self.buffers[side, kind].at[pl.ds(offset, r1 - r0)]

    def add(self, part, r0, r1, block, ins, name):
        spans = [self.rows[n] for n in ins]
        edges = {r0, r1} | {e for _, s0, s1, _ in spans for e in (s0, s1) if r0 < e < r1}
        cuts = sorted(edges)
        for a, b in zip(cuts, cuts[1:]):
            total = self.part[block, pl.ds(a, b - a)]
            for kind, s0, s1, offset in spans:
                if a >= s0 and b <= s1:
                    total = total + self.buffers["recv", kind][pl.ds(offset + a - s0, b - a)].astype(F32)
            if name is None:
                self.total[pl.ds(a, b - a)] = total
            else:
                kind, s0, _, offset = self.rows[name]
                self.buffers["send", kind][pl.ds(offset + a - s0, b - a)] = total.astype(kind)

    def hidden_grad(self, i):
        rows, cols = pl.ds(i // 3 * 256, 256), pl.ds(i % 3 * 256, 256)
        grad = jnp.dot(self.cot[rows], self.w[:, cols], preferred_element_type=F32)
        self.up_out[rows, cols] = (grad * self.to_up[rows, cols]).astype(BF16)
        self.gate_out[rows, cols] = (grad * self.to_gate[rows, cols]).astype(BF16)
        self.pending.append(self.local(self.gate_out.at[rows, cols], self.gate_grad.at[rows, cols], 35 + 2 * i))
        self.pending.append(self.local(self.up_out.at[rows, cols], self.up_grad.at[rows, cols], 36 + 2 * i))

    def finish(self):
        for n in range(6):
            rows = pl.ds(n * 128, 128)
            self.down_out[:, rows] = self.total[rows].T * self.scale
        self.pending.append(self.local(self.down_out, self.down_grad, 59))


def kernel(scale, cot_hbm, gate_hbm, up_hbm, w_hbm, gate_grad, up_grad, down_grad, cot, w, part, gate, up, to_gate, to_up, ht, gate_out, up_out, total, down_out, sb, rb, sf, rf, ssem, rsem, lsem):
    refs = dict(
        cot_hbm=cot_hbm, gate_hbm=gate_hbm, up_hbm=up_hbm, w_hbm=w_hbm,
        gate_grad=gate_grad, up_grad=up_grad, down_grad=down_grad,
        cot=cot, w=w, part=part, gate=gate, up=up, to_gate=to_gate, to_up=to_up, ht=ht,
        gate_out=gate_out, up_out=up_out, total=total, down_out=down_out, lsem=lsem,
        buffers={("send", BF16): sb, ("recv", BF16): rb, ("send", F32): sf, ("recv", F32): rf},
    )
    c = Kernel(refs, scale)
    p = Tasks(c)
    c.rows = p.rows
    copies, waited, done = {}, set(), set()
    assert sorted(ORDER) == list(range(len(p.tasks)))
    for t in ORDER:
        name, needs, _, function, message = p.tasks[t]
        for need in needs:
            if need in p.message:
                if need not in waited:
                    copies[need].wait_recv()
                    waited.add(need)
            else:
                assert need in done, need
        if function:
            function()
        if message:
            m, link, _, src, dst = message
            copies[m] = pltpu.make_async_remote_copy(
                src_ref=src(),
                dst_ref=dst(),
                send_sem=ssem.at[p.message[m]],
                recv_sem=rsem.at[p.message[m]],
                device_id=c.device(link),
                device_id_type=pl.DeviceIdType.MESH,
            )
            copies[m].start()
        done.add(name)
    assert waited == set(copies), set(copies) - waited
    c.finish()
    for m in copies:
        copies[m].wait_send()
    for copy in c.pending:
        copy.wait()


def local(cotangent, gate_pre, up_pre, down_weight):
    tokens = gate_pre.shape[0] * NZ * NY
    p = Tasks(Nothing())
    messages = len(p.message)
    hbm = pl.BlockSpec(memory_space=pl.ANY)

    def body(*refs):
        kernel(0.5 / math.sqrt(tokens), *refs)

    return pl.pallas_call(
        body,
        out_shape=(
            jax.ShapeDtypeStruct((1024, 768), BF16),
            jax.ShapeDtypeStruct((1024, 768), BF16),
            jax.ShapeDtypeStruct((128, 768), F32),
        ),
        in_specs=[hbm] * 4,
        out_specs=[hbm] * 3,
        scratch_shapes=[
            pltpu.VMEM((1024, 4096), BF16),
            pltpu.VMEM((4096, 768), BF16),
            pltpu.VMEM((32, 768, 128), F32),
            pltpu.VMEM((1024, 768), BF16),
            pltpu.VMEM((1024, 768), BF16),
            pltpu.VMEM((1024, 768), F32),
            pltpu.VMEM((1024, 768), F32),
            pltpu.VMEM((768, 1024), BF16),
            pltpu.VMEM((1024, 768), BF16),
            pltpu.VMEM((1024, 768), BF16),
            pltpu.VMEM((768, 128), F32),
            pltpu.VMEM((128, 768), F32),
            pltpu.VMEM((p.total_rows[BF16], 128), BF16),
            pltpu.VMEM((p.total_rows[BF16], 128), BF16),
            pltpu.VMEM((p.total_rows[F32], 128), F32),
            pltpu.VMEM((p.total_rows[F32], 128), F32),
            pltpu.SemaphoreType.DMA((messages,)),
            pltpu.SemaphoreType.DMA((messages,)),
            pltpu.SemaphoreType.DMA((60,)),
        ],
        compiler_params=pltpu.CompilerParams(
            collective_id=0, has_side_effects=True, vmem_limit_bytes=67043328
        ),
        name="gated_backward",
    )(cotangent, gate_pre, up_pre, down_weight)


def solution(mesh):
    torus = Mesh(mesh.devices.reshape(NZ, NY, NX, 2), ("z", "y", "x", "core"))
    rows, columns = ("z", "y"), ("x", "core")
    return jax.shard_map(
        local,
        mesh=torus,
        in_specs=(P(rows + columns, None), P(rows, columns), P(rows, columns), P(rows, columns)),
        out_specs=(P(rows, columns), P(rows, columns), P(rows, columns)),
        check_vma=False,
    )
```

time: 295 us -> 89.5 us (0.30)
  waiting for transfers between devices: 250 us -> 0 us
  Pallas kernels: 0 us -> 83.4 us
  matrix products: 26.7 us -> 0 us
  between operations: 15.2 us -> 0.65 us
  local copies, waits for them, and re-layouts: 0.92 us -> 4.75 us
    reduce_scatter x2 -> x0, waiting for transfers between devices: 142 us -> none  [sum_by_axis(): total = lax.psum_scatter(total, axis, scatter_dimension=0, tiled=True)]
    all_gather x2 -> x0, waiting for transfers between devices: 107 us -> none  [the longest x1 57 us: local(): gathered = lax.all_gather(cotangent, 'tp', axis=0, tiled=True)]
    pallas_call x0 -> x1, Pallas kernels: none -> 83.4 us  [local(): pl.pallas_call(body, out_shape=(jax.ShapeDtypeStruct((1024, 768), BF16),...]
    dot_general x2 -> x0, matrix products: 26.7 us -> none  [the longest x1 13.7 us: local(): lax.dot_general(columns, hidden, (((0,), (0,)), ((), ())), preferred_elem...]
    unnamed x5 -> x7, local copies, waits for them, and re-layouts: 0.92 us -> 4.75 us
  transfers between devices with their start and end apart: 4 -> 0, of which waited for: 3 -> 0; matrix products, arithmetic and copies ran while one was open for 4% -> 0% of each run, Pallas kernels for 0% -> 0%
where the time goes in v1:
time: 89.5 us; the launch traced here: 88.8 us
  Pallas kernels  83.4 us (93%)
  local copies, waits for them, and re-layouts  4.75 us (5%)
    pallas_call x1, Pallas kernels, local(): pl.pallas_call(body, out_shape=(jax.ShapeDtypeStruct((1024, 768), BF16),...  83.4 us
    unnamed x7, local copies, waits for them, and re-layouts  4.75 us

profile of v1, /device:TPU:8, one launch (start us, length us, event | category | flops | bytes accessed | tf_op | source)
XLA Modules:
  0.0 88.8 jit_solution(9230603968078776320)
XLA Ops:
  0.6 83.4 %gated_backward.1 = (bf16[1024,768]{1,0:T(8,128)(2,1)}, bf16[1024,768]{1,0:T(8,128)(2,1)}, f32[128,768]{1,0:T(8,128)}) custom-call(bf16[128,4096]{1,0:T(8,128)(2,1)} %refs_0_.1, bf16[1024,768]{1,0:T(8,128)(2,1)} %refs_1_.1, bf16[1024,768]{1,0:T(8,128)(2,1)} %refs_2_.1, bf16[128,768]{1,0:T(8,128)(2,1)} %refs_3_.1), custom_call_target="tpu_custom_call" | custom-call | tf_op jit(solution)/shard_map/gated_backward/pallas_call | solution.py:371
  84.1 0.0 copy-start
  84.1 2.8 %copy.10 = bf16[1024,768]{1,0:T(8,128)(2,1)} copy(bf16[1024,768]{1,0:T(8,128)(2,1)} %get-tuple-element.6) | data formatting | bytes 3145728
  86.9 0.0 copy-done
  86.9 0.0 copy-start.1
  86.9 1.1 %copy.11 = bf16[1024,768]{1,0:T(8,128)(2,1)} copy(bf16[1024,768]{1,0:T(8,128)(2,1)S(1)} %copy-done) | data formatting | bytes 3145728
  88.0 0.1 copy-done.1
  88.1 0.7 copy.12
Async XLA Ops:
  84.1 2.8 %copy-start = (bf16[1024,768]{1,0:T(8,128)(2,1)S(1)}, bf16[1024,768]{1,0:T(8,128)(2,1)}, u32[]{:S(2)}) copy-start(bf16[1024,768]{1,0:T(8,128)(2,1)} %get-tuple-element.7) | copy-start | bytes 4718596
  86.9 1.2 %copy-start.1 = (f32[128,768]{1,0:T(8,128)S(1)}, f32[128,768]{1,0:T(8,128)}, u32[]{:S(2)}) copy-start(f32[128,768]{1,0:T(8,128)} %get-tuple-element.8) | copy-start | bytes 1179652

commit v2 on v1

v2 whole, which is shorter than its diff:
```python
import math

import jax
import jax.numpy as jnp
from jax import lax
from jax.experimental import pallas as pl
from jax.experimental.pallas import tpu as pltpu
from jax.sharding import Mesh
from jax.sharding import PartitionSpec as P

ORDER = [
    0, 39, 77, 78, 82, 59, 1, 86, 87, 21, 107, 96, 97, 106, 35, 5, 43, 117, 73, 116, 88, 92, 65, 27, 60, 22,
    69, 31, 9, 40, 47, 2, 7, 45, 74, 36, 44, 6, 80, 84, 98, 102, 61, 23, 48, 10, 66, 28, 70, 32, 51, 13, 49,
    11, 41, 3, 90, 94, 79, 83, 46, 8, 62, 24, 89, 93, 67, 29, 52, 14, 71, 37, 100, 104, 108, 112, 50, 12, 75,
    33, 17, 55, 53, 15, 81, 85, 42, 4, 63, 25, 119, 185, 95, 91, 118, 180, 181, 154, 135, 131, 171, 103, 177,
    99, 188, 178, 159, 130, 120, 197, 121, 136, 193, 194, 160, 143, 142, 196, 172, 155, 54, 186, 109, 113,
    114, 110, 147, 167, 187, 148, 156, 182, 173, 166, 189, 179, 101, 105, 161, 132, 190, 19, 137, 38, 57, 64,
    144, 123, 111, 122, 195, 115, 149, 72, 34, 30, 68, 211, 26, 208, 76, 157, 212, 124, 223, 184, 125, 138,
    133, 198, 215, 225, 209, 174, 168, 204, 20, 183, 56, 201, 150, 191, 213, 210, 145, 162, 226, 202, 218,
    158, 217, 199, 227, 222, 200, 134, 206, 16, 139, 232, 192, 203, 205, 151, 169, 18, 58, 163, 229, 146, 220,
    216, 233, 214, 224, 219, 140, 234, 175, 230, 207, 141, 170, 128, 152, 164, 231, 127, 228, 221, 153, 129,
    165, 126, 235, 176,
]

NZ, NY, NX = 8, 4, 4
F32, BF16 = jnp.float32, jnp.bfloat16
BOTH = (1, -1)
ZORDER = [4, 3, -3, 2, -2, 1, -1, 0]
YORDER = [2, 1, -1, 0]
WA = 48
GA, GA_CUT, GB_CUT = 336, 176, 560
GROWS = {("A", 0): (0, GA_CUT), ("A", 1): (GA_CUT, GA), ("B", 0): (GA, GB_CUT), ("B", 1): (GB_CUT, 768)}
LINKS = [(a, s) for a in "zyx" for s in BOTH] + [("c", 1)]
BARRIER = len(LINKS)
OUTPUTS = [((1024, 768), BF16), ((1024, 768), BF16), ((128, 768), F32)]
LIMIT = 58 << 20


def nz(v):
    return (v + 3) % 8 - 3


def ny(v):
    return (v + 1) % 4 - 1


def block_at(rz, ry):
    return ZORDER.index(nz(rz)) * 4 + YORDER.index(ny(ry))


def grows(part, half):
    if half is None:
        return GROWS[part, 0][0], GROWS[part, 1][1]
    return GROWS[part, half]


def step(rz, ry, axis, sign):
    return (nz(rz - sign), ry) if axis == "z" else (rz, ny(ry - sign))


def send_group(message):
    return "WC".find(message[0]) if message[0] in "WC" else 2


def receive_group(message):
    if message[0] == "W":
        _, part, axis, _, rz, ry = message
        return ("W",) if (part, axis, ry) == ("B", "y", 2) or (part, axis, rz) == ("A", "z", 4) else message
    if message[0] == "C":
        return ("C", message[2]) if message[3][0] == "c" else message
    cls, _, s, rz, ry = message
    if cls in ("A2", "B1") and ry == 0 or cls != "B1" and rz == 0 and (cls, ry) != ("A2", 1) and (cls, ry) != ("A2", -1):
        return (cls, rz, ry)
    if abs(rz) == 2 and cls in ("A1", "B2"):
        return (cls, s, rz, ry)
    return message


def encode(value):
    value = value * 2.0**38
    return (value * jnp.abs(value)).astype(BF16)


def decode(coded):
    coded = coded.astype(F32)
    root = jnp.sqrt(jnp.abs(coded)) * 2.0**-38
    return jnp.where(coded < 0, -root, root)


class Tasks:
    def __init__(self, c):
        self.c = c
        self.tasks = []
        self.message = {}
        self.index = {}
        self.rows = {}
        self.total_rows = 0
        self.sent = [0, 0, 0]
        self.groups, self.group_size = {}, {}
        self.build()

    def task(self, name, needs, time, function=None, message=None):
        assert name not in self.index, name
        self.index[name] = len(self.tasks)
        if message:
            assert message[0] not in self.message
            self.message[message[0]] = len(self.message)
            self.sent[send_group(message[0])] += message[2] // 2
            key = receive_group(message[0])
            self.groups.setdefault(key, len(self.groups))
            self.group_size[key] = self.group_size.get(key, 0) + message[2] // 2
        self.tasks.append((name, tuple(needs), time, function, message))

    def weight(self, rz, ry, part, half, axis, sign, needs):
        tz, ty = step(rz, ry, axis, sign)
        r0, r1 = (0, WA) if part == "A" else (WA, 128)
        c0, c1 = (0, 768) if half is None else ((0, 384), (384, 768))[half]

        def at(z, y):
            b = block_at(z, y) * 128
            return lambda: self.c.w.at[pl.ds(b + r0, r1 - r0), pl.ds(c0, c1 - c0)]

        name = ("W", part, axis, sign, tz, ty)
        link, size = (axis, sign), (r1 - r0) * (c1 - c0) * 2
        self.task(("t",) + name, needs, 0.0, None, (name, link, size, at(rz, ry), at(tz, ty)))

    def cot(self, kind, piece, link, dx, half, needs):
        c = self.c
        h0, h1 = (0, 128) if half is None else ((0, 64), (64, 128))[half]

        def at():
            return c.cot.at[pl.ds(c.token_row(dx) + h0, h1 - h0), pl.ds(piece * 1024, 1024)]

        name = ("C", kind, piece, link)
        self.task(("t",) + name, needs, 0.0, None, (name, link, (h1 - h0) * 2048, at, at))

    def gradient(self, cls, part, half, axis, sign, rz, ry, needs, ins):
        c = self.c
        tz, ty = step(rz, ry, axis, sign)
        name = (cls, half, sign, tz, ty)
        r0, r1 = grows(part, half)
        self.rows[name] = (r0, r1, self.total_rows)
        self.total_rows += r1 - r0
        self.task(
            ("t",) + name,
            list(needs) + list(ins),
            0.03,
            lambda: c.add(part, r0, r1, block_at(rz, ry), ins, name),
            (name, (axis, sign), (r1 - r0) * 256, lambda: c.slot("send", name), lambda: c.slot("recv", name)),
        )

    def build(self):
        c, weight, cot, task, gradient = self.c, self.weight, self.cot, self.task, self.gradient
        task("start", [], 4.0, lambda: c.start())
        start = ["start"]
        arrived = []
        for s in BOTH:
            h = 0 if s == 1 else 1
            weight(0, 0, "B", None, "z", s, start)
            for hop in (1, 2, 3):
                weight(-s * hop, 0, "B", h if hop == 3 else None, "z", s, [("W", "B", "z", s, -s * hop, 0)])
            for rz in [0, -1, 1, -2, 2, -3, 3, 4]:
                if rz == 0:
                    needs = start
                elif rz == 4:
                    needs = [("W", "B", "z", t, 4, 0) for t in BOTH]
                else:
                    needs = [("W", "B", "z", 1 if rz < 0 else -1, rz, 0)]
                weight(rz, 0, "B", None, "y", s, needs)
                weight(rz, -s, "B", h, "y", s, [("W", "B", "y", s, rz, -s)])
                arrived.append(("W", "B", "y", s, rz, 2))
            weight(0, 0, "A", None, "y", s, start)
            weight(0, -s, "A", h, "y", s, [("W", "A", "y", s, 0, -s)])
            for ry in YORDER:
                if ry == 0:
                    needs = start
                elif ry == 2:
                    needs = [("W", "A", "y", t, 0, 2) for t in BOTH]
                else:
                    needs = [("W", "A", "y", -ry, 0, ry)]
                weight(0, ry, "A", None, "z", s, needs)
                for hop in (1, 2, 3):
                    weight(-s * hop, ry, "A", h if hop == 3 else None, "z", s, [("W", "A", "z", s, -s * hop, ry)])
                arrived.append(("W", "A", "z", s, 4, ry))
        for k in range(4):
            task(("load", k), start, 0.0, lambda k=k: c.wait_cot_load(k))
            for s in BOTH:
                h = 0 if s == 1 else 1
                own = ("C", "own", k, ("x", s))
                cot("own", k, ("x", s), 0, None, [("load", k)])
                cot("forward", k, ("x", s), -s, h, [own])
                cot("side%d" % s, k, ("c", 1), -s, None, [own])
                cot("far%d" % s, k, ("c", 1), -2 * s, h, [("C", "forward", k, ("x", s))])
            cot("own", k, ("c", 1), 0, None, [("load", k)])
        task("hidden", start, 2.0, lambda: c.hidden())
        for i, rz in enumerate(ZORDER):
            k = i // 2
            pieces = [("C", kind, k, ("c", 1)) for kind in ("own", "side1", "side-1", "far1", "far-1")]
            pieces += [("C", kind, k, ("x", s)) for kind in ("own", "forward") for s in BOTH]
            task(("down", rz), ["hidden", ("load", k)] + pieces, 1.0, lambda i=i: c.down_product(i))
        for i in range(4):
            task(("hg", i), arrived + [("down", rz) for rz in (4, -3, -2, 0)], 2.1, lambda i=i: c.hidden_grad(i))
        for ry in YORDER:
            for s in BOTH:
                h = 0 if s == 1 else 1
                gradient("A1", "A", h, "z", s, 4, ry, [("down", 4)], [])
                gradient("A1", "A", 1 - h, "z", s, 3 * s, ry, [("down", 3 * s)], [])
                gradient("A1", "A", h, "z", s, 3 * s, ry, [("down", 3 * s)], [("A1", h, s, 3 * s, ry)])
                gradient("A1", "A", None, "z", s, 2 * s, ry, [("down", 2 * s)], [("A1", v, s, 2 * s, ry) for v in (0, 1)])
                gradient("A1", "A", None, "z", s, s, ry, [("down", s)], [("A1", None, s, s, ry)])
            ins = [("A1", None, s, 0, ry) for s in BOTH]
            if ry == 2:
                for s in BOTH:
                    gradient("A2", "A", 0 if s == 1 else 1, "y", s, 0, 2, [("down", 0)], ins)
            elif ry:
                h = 0 if ry == 1 else 1
                gradient("A2", "A", 1 - h, "y", ry, 0, ry, [("down", 0)], ins)
                gradient("A2", "A", h, "y", ry, 0, ry, [("down", 0)], ins + [("A2", h, ry, 0, ry)])
            else:
                ins = ins + [("A2", v, s, 0, 0) for s in BOTH for v in (0, 1)]
                task("finalA", ins + [("down", 0)], 0.05, lambda ins=ins: c.add("A", *grows("A", None), block_at(0, 0), ins, None))
        for rz in ZORDER:
            for s in BOTH:
                h = 0 if s == 1 else 1
                gradient("B1", "B", h, "y", s, rz, 2, [("down", rz)], [])
                gradient("B1", "B", 1 - h, "y", s, rz, s, [("down", rz)], [])
                gradient("B1", "B", h, "y", s, rz, s, [("down", rz)], [("B1", h, s, rz, s)])
            ins = [("B1", v, s, rz, 0) for s in BOTH for v in (0, 1)]
            if rz == 4:
                for s in BOTH:
                    gradient("B2", "B", 0 if s == 1 else 1, "z", s, 4, 0, [("down", 4)], ins)
            elif rz:
                s = 1 if rz > 0 else -1
                h = 0 if s == 1 else 1
                if abs(rz) == 3:
                    gradient("B2", "B", 1 - h, "z", s, rz, 0, [("down", rz)], ins)
                    gradient("B2", "B", h, "z", s, rz, 0, [("down", rz)], ins + [("B2", h, s, rz, 0)])
                elif abs(rz) == 2:
                    gradient("B2", "B", None, "z", s, rz, 0, [("down", rz)], ins + [("B2", v, s, rz, 0) for v in (0, 1)])
                else:
                    gradient("B2", "B", None, "z", s, rz, 0, [("down", rz)], ins + [("B2", None, s, rz, 0)])
            else:
                ins = ins + [("B2", None, s, 0, 0) for s in BOTH]
                task("finalB", ins + [("down", 0)], 0.05, lambda ins=ins: c.add("B", *grows("B", None), block_at(0, 0), ins, None))


class Nothing:
    pass


class Kernel:
    def __init__(self, refs, scale):
        self.__dict__.update(refs)
        self.scale = scale
        self.z, self.y, self.x, self.core = (lax.axis_index(a) for a in ("z", "y", "x", "core"))

    def token_row(self, dx):
        return pl.multiple_of(lax.rem(self.x + dx + NX, NX) * 256 + self.core * 128, 128)

    def device(self, link):
        axis, sign = link
        if axis == "c":
            return {"core": 1 - self.core}
        size = {"z": NZ, "y": NY, "x": NX}[axis]
        return {axis: lax.rem(getattr(self, axis) + sign + size, size)}

    def local(self, src, dst, sem):
        copy = pltpu.make_async_copy(src, dst, self.lsem.at[sem])
        copy.start()
        return copy

    def start(self):
        barrier = pltpu.get_barrier_semaphore()
        for link in LINKS:
            pl.semaphore_signal(barrier, inc=1, device_id=self.device(link), device_id_type=pl.DeviceIdType.MESH)
        w_load = self.local(self.w_hbm, self.w.at[pl.ds(block_at(0, 0) * 128, 128)], 0)
        own = self.token_row(0)
        for i, rz in enumerate(ZORDER):
            for j, ry in enumerate(YORDER):
                col = (lax.rem(self.z + rz + NZ, NZ) * NY + lax.rem(self.y + ry + NY, NY)) * 128
                b = i * 4 + j
                source = self.cot_hbm.at[:, pl.ds(pl.multiple_of(col, 128), 128)]
                self.local(source, self.cot.at[pl.ds(own, 128), pl.ds(b * 128, 128)], 3 + b // 8)
        self.g_load = self.local(self.gate_hbm, self.gate, 1)
        self.u_load = self.local(self.up_hbm, self.up, 2)
        pl.semaphore_wait(barrier, BARRIER)
        w_load.wait()

    def wait_cot_load(self, k):
        piece = self.cot.at[pl.ds(0, 128), pl.ds(k * 1024, 1024)]
        pltpu.make_async_copy(piece, piece, self.lsem.at[3 + k]).wait()

    def hidden(self):
        self.g_load.wait()
        self.u_load.wait()

        def body(i, carry):
            rows = pl.ds(pl.multiple_of(i * 128, 128), 128)
            for n in range(6):
                cols = pl.ds(n * 128, 128)
                g = self.gate[rows, cols].astype(F32)
                u = self.up[rows, cols].astype(F32)
                s = jax.nn.sigmoid(g)
                silu = g * s
                self.ht[cols, rows] = (silu * u).T.astype(BF16)
                self.to_up[rows, cols] = 0.5 * silu
                self.to_gate[rows, cols] = 0.5 * (u * s * (1.0 + g * (1.0 - s)))
            return carry

        lax.fori_loop(0, 8, body, 0)

    def down_product(self, z):
        for half in range(2):
            b = z * 4 + half * 2
            res = jnp.dot(self.ht[...], self.cot[:, pl.ds(b * 128, 256)], preferred_element_type=F32)
            self.part[b] = res[:, :128]
            self.part[b + 1] = res[:, 128:]

    def slot(self, side, name):
        r0, r1, offset = self.rows[name]
        return self.buffers[side].at[pl.ds(offset, r1 - r0)]

    def add(self, part, r0, r1, block, ins, name):
        spans = [self.rows[n] for n in ins]
        edges = {r0, r1} | {e for s0, s1, _ in spans for e in (s0, s1) if r0 < e < r1}
        cuts = sorted(edges)
        for a, b in zip(cuts, cuts[1:]):
            total = self.part[block, pl.ds(a, b - a)]
            for s0, s1, offset in spans:
                if a >= s0 and b <= s1:
                    total = total + decode(self.buffers["recv"][pl.ds(offset + a - s0, b - a)])
            if name is None:
                self.total[pl.ds(a, b - a)] = total
            else:
                s0, _, offset = self.rows[name]
                self.buffers["send"][pl.ds(offset + a - s0, b - a)] = encode(total)

    def hidden_grad(self, i):
        def multiply(j, carry):
            rows = pl.ds(pl.multiple_of(i * 256 + j * 128, 128), 128)
            for n in range(3):
                cols = pl.ds(n * 256, 256)
                here = pl.ds(pl.multiple_of(j * 128, 128), 128)
                self.acc[here, cols] = jnp.dot(self.cot[rows], self.w[:, cols], preferred_element_type=F32)
            return carry

        def finish(j, carry):
            rows = pl.ds(pl.multiple_of(i * 256 + j * 32, 32), 32)
            grad = self.acc[pl.ds(pl.multiple_of(j * 32, 32), 32)]
            self.up_out[rows] = (grad * self.to_up[rows]).astype(BF16)
            self.gate_out[rows] = (grad * self.to_gate[rows]).astype(BF16)
            return carry

        lax.fori_loop(0, 2, multiply, 0)
        lax.fori_loop(0, 8, finish, 0, unroll=2)

    def finish(self):
        for n in range(6):
            rows = pl.ds(n * 128, 128)
            self.down_out[:, rows] = self.total[rows].T * self.scale


def kernel(scale, cot_hbm, gate_hbm, up_hbm, w_hbm, gate_out, up_out, down_out, cot, w, part, gate, up, to_gate, to_up, ht, acc, total, sb, rb, ssem, rsem, lsem):
    refs = dict(
        cot_hbm=cot_hbm, gate_hbm=gate_hbm, up_hbm=up_hbm, w_hbm=w_hbm,
        cot=cot, w=w, part=part, gate=gate, up=up, to_gate=to_gate, to_up=to_up, ht=ht,
        gate_out=gate_out, up_out=up_out, acc=acc, total=total, down_out=down_out, lsem=lsem,
        buffers={"send": sb, "recv": rb},
    )
    c = Kernel(refs, scale)
    p = Tasks(c)
    c.rows = p.rows
    waited, sent, done = set(), set(), set()
    assert sorted(ORDER) == list(range(len(p.tasks)))

    def all_of(kind, elements):
        ref = {"W": w, "C": cot}.get(kind, rb)
        assert elements % ref.shape[1] == 0
        return ref.at[pl.ds(0, elements // ref.shape[1])]

    def remote(src, dst, send, receive, link):
        return pltpu.make_async_remote_copy(
            src_ref=src,
            dst_ref=dst,
            send_sem=ssem.at[send],
            recv_sem=rsem.at[receive],
            device_id=c.device(link),
            device_id_type=pl.DeviceIdType.MESH,
        )

    for t in ORDER:
        name, needs, _, function, message = p.tasks[t]
        for need in needs:
            if need in p.message:
                key = receive_group(need)
                if key not in waited:
                    assert all(m in sent for m in p.message if receive_group(m) == key)
                    ref = all_of(need[0], p.group_size[key])
                    remote(ref, ref, 0, p.groups[key], LINKS[0]).wait_recv()
                    waited.add(key)
            else:
                assert need in done, need
        if function:
            function()
        if message:
            m, link, _, src, dst = message
            remote(src(), dst(), send_group(m), p.groups[receive_group(m)], link).start()
            sent.add(m)
        done.add(name)
    assert waited == set(p.groups), set(p.groups) - waited
    c.finish()
    for i, kind in enumerate("WCG"):
        ref = all_of(kind, p.sent[i])
        remote(ref, ref, i, 0, LINKS[0]).wait_send()


def copy_out(gate_in, up_in, down_in, gate_grad, up_grad, down_grad, sem):
    pairs = [(gate_in, gate_grad), (up_in, up_grad), (down_in, down_grad)]
    copies = [pltpu.make_async_copy(src, dst, sem.at[i]) for i, (src, dst) in enumerate(pairs)]
    for copy in copies:
        copy.start()
    for copy in copies:
        copy.wait()


def local(cotangent, gate_pre, up_pre, down_weight):
    tokens = gate_pre.shape[0] * NZ * NY
    p = Tasks(Nothing())
    hbm = pl.BlockSpec(memory_space=pl.ANY)

    def body(*refs):
        kernel(0.5 / math.sqrt(tokens), *refs)

    results = pl.pallas_call(
        body,
        out_shape=tuple(pltpu.VMEM(*o) for o in OUTPUTS),
        in_specs=[hbm] * 4,
        out_specs=[pl.BlockSpec(memory_space=pltpu.VMEM)] * 3,
        scratch_shapes=[
            pltpu.VMEM((1024, 4096), BF16),
            pltpu.VMEM((4096, 768), BF16),
            pltpu.VMEM((32, 768, 128), F32),
            pltpu.VMEM((1024, 768), BF16),
            pltpu.VMEM((1024, 768), BF16),
            pltpu.VMEM((1024, 768), F32),
            pltpu.VMEM((1024, 768), F32),
            pltpu.VMEM((768, 1024), BF16),
            pltpu.VMEM((256, 768), F32),
            pltpu.VMEM((768, 128), F32),
            pltpu.VMEM((p.total_rows, 128), BF16),
            pltpu.VMEM((p.total_rows, 128), BF16),
            pltpu.SemaphoreType.DMA((3,)),
            pltpu.SemaphoreType.DMA((len(p.groups),)),
            pltpu.SemaphoreType.DMA((7,)),
        ],
        compiler_params=pltpu.CompilerParams(
            collective_id=0, has_side_effects=True, vmem_limit_bytes=LIMIT
        ),
        name="gated_backward",
    )(cotangent, gate_pre, up_pre, down_weight)
    return pl.pallas_call(
        copy_out,
        out_shape=tuple(jax.ShapeDtypeStruct(*o) for o in OUTPUTS),
        in_specs=[pl.BlockSpec(memory_space=pltpu.VMEM)] * 3,
        out_specs=[hbm] * 3,
        scratch_shapes=[pltpu.SemaphoreType.DMA((3,))],
        compiler_params=pltpu.CompilerParams(vmem_limit_bytes=1 << 20),
        name="copy_out",
    )(*results)


def solution(mesh):
    torus = Mesh(mesh.devices.reshape(NZ, NY, NX, 2), ("z", "y", "x", "core"))
    rows, columns = ("z", "y"), ("x", "core")
    return jax.shard_map(
        local,
        mesh=torus,
        in_specs=(P(rows + columns, None), P(rows, columns), P(rows, columns), P(rows, columns)),
        out_specs=(P(rows, columns), P(rows, columns), P(rows, columns)),
        check_vma=False,
    )
```

time: 89.5 us -> 83.4 us (0.932)
  local copies, waits for them, and re-layouts: 4.75 us -> 0 us
  Pallas kernels: 83.4 us -> 82.5 us
    unnamed x7 -> x0, local copies, waits for them, and re-layouts: 4.75 us -> none
    pallas_call x1 -> x2, Pallas kernels: 83.4 us -> 82.5 us  [the longest x1 80.7 us: local(): pl.pallas_call(body, out_shape=tuple((pltpu.VMEM(*o) for o in OUTPUTS)),...]
where the time goes in v2:
time: 83.4 us; the launch traced here: 83.3 us
  Pallas kernels  82.5 us (99%)
    pallas_call x1, Pallas kernels, local(): pl.pallas_call(body, out_shape=tuple((pltpu.VMEM(*o) for o in OUTPUTS)),...  80.7 us
    pallas_call x1, Pallas kernels, local(): pl.pallas_call(copy_out, out_shape=tuple((jax.ShapeDtypeStruct(*o) for o...  1.81 us

profile of v2, /device:TPU:8, one launch (start us, length us, event | category | flops | bytes accessed | tf_op | source)
XLA Modules:
  0.0 83.3 jit_solution(10364036520654013185)
XLA Ops:
  0.6 80.7 %gated_backward.1 = (bf16[1024,768]{1,0:T(8,128)(2,1)S(1)}, bf16[1024,768]{1,0:T(8,128)(2,1)S(1)}, f32[128,768]{1,0:T(8,128)S(1)}) custom-call(bf16[128,4096]{1,0:T(8,128)(2,1)} %refs_0_.1, bf16[1024,768]{1,0:T(8,128)(2,1)} %refs_1_.1, bf16[1024,768]{1,0:T(8,128)(2,1)} %refs_2_.1, bf16[128,768]{1,0:T(8,128)(2,1)} %refs_3_.1), custom_call_target="tpu_custom_call" | custom-call | tf_op jit(solution)/shard_map/gated_backward/pallas_call | solution.py:434
  81.3 1.8 %copy_out.1 = (bf16[1024,768]{1,0:T(8,128)(2,1)}, bf16[1024,768]{1,0:T(8,128)(2,1)}, f32[128,768]{1,0:T(8,128)}) custom-call(bf16[1024,768]{1,0:T(8,128)(2,1)S(1)} %get-tuple-element.6.gate_in, bf16[1024,768]{1,0:T(8,128)(2,1)S(1)} %get-tuple-element.7.up_in, f32[128,768]{1,0:T(8,128)S(1)} %get-tuple-element.8.down_in), custom_call_target="tpu_custom_call" | custom-call | tf_op jit(solution)/shard_map/copy_out/pallas_call | solution.py:461

commit v3 on v2

--- a/solution.py
+++ b/solution.py
@@ -9,17 +9,17 @@
 from jax.sharding import PartitionSpec as P
 
 ORDER = [
-    0, 39, 77, 78, 82, 59, 1, 86, 87, 21, 107, 96, 97, 106, 35, 5, 43, 117, 73, 116, 88, 92, 65, 27, 60, 22,
-    69, 31, 9, 40, 47, 2, 7, 45, 74, 36, 44, 6, 80, 84, 98, 102, 61, 23, 48, 10, 66, 28, 70, 32, 51, 13, 49,
-    11, 41, 3, 90, 94, 79, 83, 46, 8, 62, 24, 89, 93, 67, 29, 52, 14, 71, 37, 100, 104, 108, 112, 50, 12, 75,
-    33, 17, 55, 53, 15, 81, 85, 42, 4, 63, 25, 119, 185, 95, 91, 118, 180, 181, 154, 135, 131, 171, 103, 177,
-    99, 188, 178, 159, 130, 120, 197, 121, 136, 193, 194, 160, 143, 142, 196, 172, 155, 54, 186, 109, 113,
-    114, 110, 147, 167, 187, 148, 156, 182, 173, 166, 189, 179, 101, 105, 161, 132, 190, 19, 137, 38, 57, 64,
-    144, 123, 111, 122, 195, 115, 149, 72, 34, 30, 68, 211, 26, 208, 76, 157, 212, 124, 223, 184, 125, 138,
-    133, 198, 215, 225, 209, 174, 168, 204, 20, 183, 56, 201, 150, 191, 213, 210, 145, 162, 226, 202, 218,
-    158, 217, 199, 227, 222, 200, 134, 206, 16, 139, 232, 192, 203, 205, 151, 169, 18, 58, 163, 229, 146, 220,
-    216, 233, 214, 224, 219, 140, 234, 175, 230, 207, 141, 170, 128, 152, 164, 231, 127, 228, 221, 153, 129,
-    165, 126, 235, 176,
+    0, 1, 97, 77, 82, 78, 107, 21, 39, 87, 96, 59, 5, 86, 106, 35, 117, 43, 116, 73, 112, 88, 31, 69, 22, 65,
+    27, 60, 2, 7, 45, 40, 9, 47, 36, 74, 6, 44, 84, 80, 102, 79, 23, 61, 8, 28, 66, 46, 98, 32, 70, 49, 11,
+    13, 51, 3, 41, 114, 90, 92, 10, 48, 24, 75, 81, 108, 29, 62, 12, 50, 37, 71, 104, 83, 14, 33, 67, 52, 15,
+    53, 17, 100, 4, 113, 89, 55, 42, 25, 76, 63, 94, 93, 99, 30, 38, 72, 16, 34, 85, 110, 54, 68, 103, 109,
+    19, 57, 118, 135, 154, 56, 177, 180, 91, 119, 185, 188, 130, 18, 147, 115, 159, 143, 155, 166, 171, 64,
+    142, 186, 181, 95, 101, 167, 178, 189, 156, 20, 58, 120, 137, 149, 136, 179, 105, 132, 160, 196, 121, 194,
+    161, 197, 131, 26, 111, 148, 123, 193, 182, 144, 172, 168, 122, 211, 187, 124, 190, 201, 173, 138, 157,
+    125, 216, 133, 225, 162, 198, 126, 150, 183, 195, 208, 218, 204, 145, 128, 184, 213, 203, 191, 139, 215,
+    205, 158, 209, 129, 199, 134, 222, 227, 163, 202, 212, 127, 192, 210, 200, 223, 206, 219, 146, 151, 220,
+    217, 169, 226, 174, 229, 232, 224, 141, 230, 207, 164, 214, 140, 233, 152, 170, 231, 175, 234, 165, 221,
+    228, 153, 176, 235,
 ]
 
 NZ, NY, NX = 8, 4, 4
@@ -144,7 +144,7 @@
         self.task(
             ("t",) + name,
             list(needs) + list(ins),
-            0.03,
+            0.05,
             lambda: c.add(part, r0, r1, block_at(rz, ry), ins, name),
             (name, (axis, sign), (r1 - r0) * 256, lambda: c.slot("send", name), lambda: c.slot("recv", name)),
         )

time: 83.4 us -> 82.2 us (0.986)
  Pallas kernels: 82.5 us -> 81.3 us
    pallas_call x1, Pallas kernels: 80.7 us -> 79.5 us  [local(): pl.pallas_call(body, out_shape=tuple((pltpu.VMEM(*o) for o in OUTPUTS)),...]
where the time goes in v3:
time: 82.2 us; the launch traced here: 82.1 us
  Pallas kernels  81.3 us (99%)
    pallas_call x1, Pallas kernels, local(): pl.pallas_call(body, out_shape=tuple((pltpu.VMEM(*o) for o in OUTPUTS)),...  79.5 us
    pallas_call x1, Pallas kernels, local(): pl.pallas_call(copy_out, out_shape=tuple((jax.ShapeDtypeStruct(*o) for o...  1.81 us

profile of v3, /device:TPU:8, one launch (start us, length us, event | category | flops | bytes accessed | tf_op | source)
XLA Modules:
  0.0 82.1 jit_solution(14792332783574837345)
XLA Ops:
  0.6 79.5 %gated_backward.1 = (bf16[1024,768]{1,0:T(8,128)(2,1)S(1)}, bf16[1024,768]{1,0:T(8,128)(2,1)S(1)}, f32[128,768]{1,0:T(8,128)S(1)}) custom-call(bf16[128,4096]{1,0:T(8,128)(2,1)} %refs_0_.1, bf16[1024,768]{1,0:T(8,128)(2,1)} %refs_1_.1, bf16[1024,768]{1,0:T(8,128)(2,1)} %refs_2_.1, bf16[128,768]{1,0:T(8,128)(2,1)} %refs_3_.1), custom_call_target="tpu_custom_call" | custom-call | tf_op jit(solution)/shard_map/gated_backward/pallas_call | solution.py:434
  80.2 1.8 %copy_out.1 = (bf16[1024,768]{1,0:T(8,128)(2,1)}, bf16[1024,768]{1,0:T(8,128)(2,1)}, f32[128,768]{1,0:T(8,128)}) custom-call(bf16[1024,768]{1,0:T(8,128)(2,1)S(1)} %get-tuple-element.6.gate_in, bf16[1024,768]{1,0:T(8,128)(2,1)S(1)} %get-tuple-element.7.up_in, f32[128,768]{1,0:T(8,128)S(1)} %get-tuple-element.8.down_in), custom_call_target="tpu_custom_call" | custom-call | tf_op jit(solution)/shard_map/copy_out/pallas_call | solution.py:461

commit v4 on v3

--- a/solution.py
+++ b/solution.py
@@ -65,7 +65,8 @@
 def receive_group(message):
     if message[0] == "W":
         _, part, axis, _, rz, ry = message
-        return ("W",) if (part, axis, ry) == ("B", "y", 2) or (part, axis, rz) == ("A", "z", 4) else message
+        last = (part, axis, ry) == ("B", "y", 2) or (part, axis, rz) == ("A", "z", 4)
+        return ("W",) if last else ("W", part, axis, abs(rz) if axis == "z" else rz, abs(ry) if axis == "y" else ry)
     if message[0] == "C":
         return ("C", message[2]) if message[3][0] == "c" else message
     cls, _, s, rz, ry = message
@@ -98,6 +99,10 @@
         self.sent = [0, 0, 0]
         self.groups, self.group_size = {}, {}
         self.build()
+        for i, (name, needs, *rest) in enumerate(self.tasks):
+            keys = {receive_group(n) for n in needs if n in self.message}
+            whole = [m for m in self.message if receive_group(m) in keys]
+            self.tasks[i] = (name, tuple(n for n in needs if n not in self.message) + tuple(whole), *rest)
 
     def task(self, name, needs, time, function=None, message=None):
         assert name not in self.index, name
@@ -274,6 +279,11 @@
         for link in LINKS:
             pl.semaphore_signal(barrier, inc=1, device_id=self.device(link), device_id_type=pl.DeviceIdType.MESH)
         w_load = self.local(self.w_hbm, self.w.at[pl.ds(block_at(0, 0) * 128, 128)], 0)
+        self.load_cot()
+        pl.semaphore_wait(barrier, BARRIER)
+        w_load.wait()
+
+    def load_cot(self):
         own = self.token_row(0)
         for i, rz in enumerate(ZORDER):
             for j, ry in enumerate(YORDER):
@@ -283,8 +293,6 @@
                 self.local(source, self.cot.at[pl.ds(own, 128), pl.ds(b * 128, 128)], 3 + b // 8)
         self.g_load = self.local(self.gate_hbm, self.gate, 1)
         self.u_load = self.local(self.up_hbm, self.up, 2)
-        pl.semaphore_wait(barrier, BARRIER)
-        w_load.wait()
 
     def wait_cot_load(self, k):
         piece = self.cot.at[pl.ds(0, 128), pl.ds(k * 1024, 1024)]
@@ -416,7 +424,12 @@
 
 def copy_out(gate_in, up_in, down_in, gate_grad, up_grad, down_grad, sem):
     pairs = [(gate_in, gate_grad), (up_in, up_grad), (down_in, down_grad)]
-    copies = [pltpu.make_async_copy(src, dst, sem.at[i]) for i, (src, dst) in enumerate(pairs)]
+    copies = []
+    for src, dst in pairs:
+        height = src.shape[0] // 4
+        for i in range(4):
+            rows = pl.ds(i * height, height)
+            copies.append(pltpu.make_async_copy(src.at[rows], dst.at[rows], sem.at[len(copies)]))
     for copy in copies:
         copy.start()
     for copy in copies:
@@ -463,7 +476,7 @@
         out_shape=tuple(jax.ShapeDtypeStruct(*o) for o in OUTPUTS),
         in_specs=[pl.BlockSpec(memory_space=pltpu.VMEM)] * 3,
         out_specs=[hbm] * 3,
-        scratch_shapes=[pltpu.SemaphoreType.DMA((3,))],
+        scratch_shapes=[pltpu.SemaphoreType.DMA((12,))],
         compiler_params=pltpu.CompilerParams(vmem_limit_bytes=1 << 20),
         name="copy_out",
     )(*results)

time: 82.2 us -> 82 us (level)
  no operation moved by 1% of the time
where the time goes in v4:
time: 82 us
  Pallas kernels  81.2 us (99%)
    pallas_call x1, Pallas kernels, local(): pl.pallas_call(body, out_shape=tuple((pltpu.VMEM(*o) for o in OUTPUTS)),...  79.3 us
    pallas_call x1, Pallas kernels, local(): pl.pallas_call(copy_out, out_shape=tuple((jax.ShapeDtypeStruct(*o) for o...  1.88 us

profile of v4, /device:TPU:8, one launch (start us, length us, event | category | flops | bytes accessed | tf_op | source)
XLA Modules:
  0.0 82.0 jit_solution(9438134957220344049)
XLA Ops:
  0.6 79.3 %gated_backward.1 = (bf16[1024,768]{1,0:T(8,128)(2,1)S(1)}, bf16[1024,768]{1,0:T(8,128)(2,1)S(1)}, f32[128,768]{1,0:T(8,128)S(1)}) custom-call(bf16[128,4096]{1,0:T(8,128)(2,1)} %refs_0_.1, bf16[1024,768]{1,0:T(8,128)(2,1)} %refs_1_.1, bf16[1024,768]{1,0:T(8,128)(2,1)} %refs_2_.1, bf16[128,768]{1,0:T(8,128)(2,1)} %refs_3_.1), custom_call_target="tpu_custom_call" | custom-call | tf_op jit(solution)/shard_map/gated_backward/pallas_call | solution.py:447
  79.9 1.9 %copy_out.1 = (bf16[1024,768]{1,0:T(8,128)(2,1)}, bf16[1024,768]{1,0:T(8,128)(2,1)}, f32[128,768]{1,0:T(8,128)}) custom-call(bf16[1024,768]{1,0:T(8,128)(2,1)S(1)} %get-tuple-element.6.gate_in, bf16[1024,768]{1,0:T(8,128)(2,1)S(1)} %get-tuple-element.7.up_in, f32[128,768]{1,0:T(8,128)S(1)} %get-tuple-element.8.down_in), custom_call_target="tpu_custom_call" | custom-call | tf_op jit(solution)/shard_map/copy_out/pallas_call | solution.py:474
